TPU v7x, 32 devices: a whole 2x2x4 slice. The times are simulated.
32 devices in a mesh: grp: 2 (over y), sp: 8 (over z, core), tp: 2 (over x).
Axes of the slice: x: 2, y: 2, z: 4, core: 2. Of those that a mesh axis runs over, the one named last changes fastest.
Arguments:
- query_plain: bfloat16 [2560, 1024], P(('grp', 'sp'), 'tp'), parts along dimension 0, may hold values from -6 to 6
- query_turn: bfloat16 [2560, 512], P(('grp', 'sp'), 'tp'), parts along dimension 0, may hold values from -40 to 40, as said below
- latent: bfloat16 [2560, 512], P(('grp', 'sp')), parts along dimension 0, may hold values from -6 to 6
- key_turn: bfloat16 [2560, 64], P(('grp', 'sp')), parts along dimension 0, may hold values from -40 to 40, as said below
- latent_norm_scale: bfloat16 [512], replicated, may hold values from 0.099609375 to 1.8984375
- plain_key_matrix: bfloat16 [512, 1024], P(None, 'tp'), may hold values from -0.25 to 0.25
- value_matrix: bfloat16 [512, 1024], P(None, 'tp'), may hold values from -0.25 to 0.25
- residual: bfloat16 [2560, 2048], P(('grp', 'sp', 'tp')), parts along dimension 0, may hold values from -6 to 6
- out_weight: bfloat16 [1024, 2048], replicated, may hold values from -6 to 6
- ffn_gain: bfloat16 [2048], replicated, may hold values from 0.099609375 to 1.8984375
- gate_weight: bfloat16 [8, 2048, 1024], P('sp', None, 'tp'), may hold values from -1 to 1
- up_weight: bfloat16 [8, 2048, 1024], P('sp', None, 'tp'), may hold values from -1 to 1
- down_weight: bfloat16 [8, 1024, 2048], P('sp', 'tp'), may hold values from -0.0625 to 0.0625
- routes: int32 [2560, 4], P(('grp', 'sp', 'tp')), parts along dimension 0, may hold values from 0 to 7, all different within a row; in each aligned block of 80 rows (0 to 79, 80 to 159, ...) at most 60 rows name the same one
- route_weights: float32 [2560, 4], P(('grp', 'sp', 'tp')), parts along dimension 0, may hold values from 0.1 to 0.6
Outputs:
- mixed: bfloat16 [2560, 2048], P(('grp', 'sp', 'tp')), parts along dimension 0
There are 2 independent parts, one for each index of `grp`. A program takes and returns all parts, laid end to end along the dimension named above; an argument that names none is the same for every part. Nothing has to cross between parts.
Inputs may be any that keep to these rules, and one draw needn't show every extreme that they name: `query_turn`: in the hidden draw some rows are large. `key_turn`: in the hidden draw some rows are large. `routes`: each row names 4 different experts. In each aligned block of 80 rows (the rows of one device) no expert is named more than 60 times, a bound that some block reaches.
All inputs are finite; a program needn't handle non-finite values.
Results may differ from a plain program's by a relative error of at most 0.015.
Values may be sent and summed in bfloat16 or wider, within the bound.
A program may use at most 128 MiB of HBM per device.

v0:
```python
import jax
import jax.numpy as jnp
from jax import lax
from jax.sharding import PartitionSpec as P

PLAIN_HEAD_WIDTH = 128
QK_ROPE = 64
VALUE_WIDTH = 128
GRID_W = 64
theta = 10000.0
eps = 1e-06
limit = 7.0
slope = 1.702


def turn(vector, row_shift, col_shift):
    width = vector.shape[-1]
    count = width // 4
    half = width // 2
    freqs = theta ** (-jnp.arange(count, dtype=jnp.float32) / count)
    extra = (1,) * (vector.ndim - 2)
    pieces = []
    for portion, shift in ((vector[..., :half], row_shift), (vector[..., half:], col_shift)):
        angle = (shift.astype(jnp.float32)[:, None] * freqs[None, :]).reshape(
            (shift.shape[0],) + extra + (count,)
        )
        lower = portion[..., :count]
        upper = portion[..., count:]
        pieces.append(
            jnp.concatenate(
                [
                    lower * jnp.cos(angle) - upper * jnp.sin(angle),
                    lower * jnp.sin(angle) + upper * jnp.cos(angle),
                ],
                axis=-1,
            )
        )
    return jnp.concatenate(pieces, axis=-1)


def norm_scale(values, gain):
    wide = values.astype(jnp.float32)
    return (
        wide
        * lax.rsqrt(jnp.mean(wide * wide, axis=-1, keepdims=True) + eps)
        * gain.astype(jnp.float32)
    )


def expert_active(rows, gate_w, up_w):
    gate_pre = jnp.minimum(jnp.dot(rows, gate_w, preferred_element_type=jnp.float32), limit)
    up_pre = jnp.clip(jnp.dot(rows, up_w, preferred_element_type=jnp.float32), -limit, limit)
    return ((up_pre + 1.0) * gate_pre * jax.nn.sigmoid(slope * gate_pre)).astype(jnp.bfloat16)


def expert_whole(rows, gate_w, up_w, down_w, groups):
    active = expert_active(rows, gate_w, up_w)
    piece = down_w.shape[0] // groups
    total = jnp.zeros((rows.shape[0], down_w.shape[1]), jnp.float32)
    for index in range(groups):
        product = jnp.dot(
            active[:, index * piece : (index + 1) * piece],
            down_w[index * piece : (index + 1) * piece],
            preferred_element_type=jnp.float32,
        )
        total = total + product.astype(jnp.bfloat16).astype(jnp.float32)
    return total.astype(jnp.bfloat16)


def on_device(
    query_plain,
    query_turn,
    latent,
    key_turn,
    latent_norm_scale,
    plain_key_matrix,
    value_matrix,
    residual,
    out_weight,
    ffn_gain,
    gate_weight,
    up_weight,
    down_weight,
    routes,
    route_weights,
):
    tok_dev = latent.shape[0]
    heads_dev = query_plain.shape[1] // PLAIN_HEAD_WIDTH
    model_width = residual.shape[1]
    place = lax.axis_index("sp") * tok_dev + jnp.arange(tok_dev, dtype=jnp.int32)
    grid_row = place // GRID_W
    grid_col = place % GRID_W
    normed_latent = norm_scale(latent, latent_norm_scale).astype(jnp.bfloat16)
    key_plain = jnp.dot(normed_latent, plain_key_matrix, preferred_element_type=jnp.float32).astype(
        jnp.bfloat16
    )
    values = jnp.dot(normed_latent, value_matrix, preferred_element_type=jnp.float32).astype(
        jnp.bfloat16
    )
    key_rot = turn(key_turn.astype(jnp.float32), grid_row, grid_col).astype(jnp.bfloat16)
    key_pairs = key_rot.reshape(tok_dev // 2, 2 * QK_ROPE)
    query_rot = turn(
        query_turn.astype(jnp.float32).reshape(tok_dev, heads_dev, QK_ROPE), grid_row, grid_col
    ).astype(jnp.bfloat16)
    plain_query = query_plain.reshape(tok_dev, heads_dev, PLAIN_HEAD_WIDTH)
    scale = (PLAIN_HEAD_WIDTH + QK_ROPE) ** (-0.5)
    most = jnp.full((heads_dev, tok_dev), -jnp.inf, jnp.float32)
    total = jnp.zeros((heads_dev, tok_dev), jnp.float32)
    summed = jnp.zeros((heads_dev, tok_dev, VALUE_WIDTH), jnp.float32)
    piece_keys = lax.all_gather(key_plain, "sp", axis=0, tiled=True)
    piece_values = lax.all_gather(values, "sp", axis=0, tiled=True)
    piece_pairs = lax.all_gather(key_pairs, "sp", axis=0, tiled=True)
    count = piece_keys.shape[0]
    piece_rot = piece_pairs.reshape(count, QK_ROPE)
    new_most = []
    new_total = []
    new_summed = []
    for head in range(heads_dev):
        head_keys = piece_keys[:, head * PLAIN_HEAD_WIDTH : (head + 1) * PLAIN_HEAD_WIDTH]
        head_values = piece_values[:, head * VALUE_WIDTH : (head + 1) * VALUE_WIDTH]
        scores = (
            jnp.einsum(
                "qd,kd->qk", plain_query[:, head], head_keys, preferred_element_type=jnp.float32
            )
            + jnp.einsum(
                "qd,kd->qk", query_rot[:, head], piece_rot, preferred_element_type=jnp.float32
            )
        ) * scale
        peak = jnp.max(scores, axis=1)
        factor = jnp.exp(most[head] - peak)
        weights = jnp.exp(scores - peak[:, None])
        new_total.append(total[head] * factor + jnp.sum(weights, axis=1))
        new_summed.append(
            summed[head] * factor[:, None]
            + jnp.dot(weights.astype(jnp.bfloat16), head_values, preferred_element_type=jnp.float32)
        )
        new_most.append(peak)
    total = jnp.stack(new_total)
    summed = jnp.stack(new_summed)
    attended = jnp.transpose((summed / total[..., None]).astype(jnp.bfloat16), (1, 0, 2)).reshape(
        tok_dev, heads_dev * VALUE_WIDTH
    )
    rows_dev = residual.shape[0]
    own_rows = lax.dynamic_slice_in_dim(
        out_weight, lax.axis_index("tp") * heads_dev * VALUE_WIDTH, heads_dev * VALUE_WIDTH, 0
    )
    projected = lax.psum_scatter(
        jnp.dot(attended, own_rows, preferred_element_type=jnp.float32).astype(jnp.bfloat16),
        "tp",
        scatter_dimension=0,
        tiled=True,
    ).astype(jnp.float32)
    hidden = (residual.astype(jnp.float32) + projected).astype(jnp.bfloat16)
    normed = norm_scale(hidden, ffn_gain).astype(jnp.bfloat16)
    top_count = routes.shape[1]
    experts_all = lax.axis_size("sp") * gate_weight.shape[0]
    capacity = min(rows_dev, max(2, rows_dev * top_count * 3 // (2 * experts_all)))
    flat_routes = routes.reshape(rows_dev * top_count)
    marks = (flat_routes[:, None] == jnp.arange(experts_all, dtype=jnp.int32)[None, :]).astype(
        jnp.int32
    )
    earlier = jnp.cumsum(marks, axis=0, dtype=jnp.int32) - marks
    slots = jnp.sum(earlier * marks, axis=1, dtype=jnp.int32)
    target = flat_routes * capacity + slots
    chosen = (
        target.reshape(rows_dev, top_count)[None, :, :]
        == jnp.arange(experts_all * capacity, dtype=jnp.int32)[:, None, None]
    )
    dispatch_table = jnp.sum(chosen.astype(jnp.bfloat16), axis=2)
    outgoing = jnp.dot(dispatch_table, normed, preferred_element_type=jnp.float32).astype(
        jnp.bfloat16
    )
    outgoing = outgoing.reshape(experts_all, capacity, model_width)
    gate_w = gate_weight[0]
    up_w = up_weight[0]
    down_w = down_weight[0]
    group = lax.axis_size("tp")
    gate_full, up_full, down_full = (
        lax.all_gather(gate_w, "tp", axis=1, tiled=True),
        lax.all_gather(up_w, "tp", axis=1, tiled=True),
        lax.all_gather(down_w, "tp", axis=0, tiled=True),
    )
    arrived = lax.all_to_all(outgoing, "sp", split_axis=0, concat_axis=0, tiled=True)
    result_rows = expert_whole(
        arrived.reshape(experts_all * capacity, model_width), gate_full, up_full, down_full, group
    )
    returned = lax.all_to_all(
        result_rows.reshape(experts_all, capacity, model_width),
        "sp",
        split_axis=0,
        concat_axis=0,
        tiled=True,
    )
    picked = returned.reshape(experts_all * capacity, model_width)[target]
    picked = picked.reshape(rows_dev, top_count, model_width).astype(jnp.float32)
    return (hidden.astype(jnp.float32) + jnp.sum(route_weights[..., None] * picked, axis=1)).astype(
        jnp.bfloat16
    )


def solution(mesh):
    placed = (
        P(("grp", "sp"), "tp"),
        P(("grp", "sp"), "tp"),
        P(("grp", "sp"), None),
        P(("grp", "sp"), None),
        P(),
        P(None, "tp"),
        P(None, "tp"),
        P(("grp", "sp", "tp"), None),
        P(),
        P(),
        P("sp", None, "tp"),
        P("sp", None, "tp"),
        P("sp", "tp", None),
        P(("grp", "sp", "tp"), None),
        P(("grp", "sp", "tp"), None),
    )
    return jax.shard_map(
        on_device,
        mesh=mesh,
        in_specs=placed,
        out_specs=P(("grp", "sp", "tp"), None),
        check_vma=False,
    )
```

profile of v0, /device:TPU:0, one launch (start us, length us, event | category | flops | bytes accessed | tf_op | source)
XLA Modules:
  0.0 335.4 jit_solution(11522728959038800007)
XLA Ops:
  6.6 1.1 fusion.38
  8.4 1.9 convolution_convert_fusion.5
  10.3 2.1 convolution_convert_fusion.4
  13.1 16.3 %all_gather.19 = bf16[640,128]{1,0:T(8,128)(2,1)S(1)} all-gather(bf16[80,128]{1,0:T(8,128)(2,1)S(1)} %convert_element_type.125), channel_id=1, replica_groups=mesh['grp'=2,'sp'=8,'tp'=2] {'sp'}, dimensions={0}, use_global_device_ids=true | all-gather | bytes 184320 | tf_op jit(solution)/shard_map/all_gather | solution.py:112
  30.0 7.3 %all-gather.9.cloned.1.call-done = bf16[1280,512]{1,0:T(8,128)(2,1)} async-done(((bf16[160,512]{1,0:T(8,128)(2,1)}), bf16[1280,512]{1,0:T(8,128)(2,1)}) %all-gather.9.cloned.1.call-update) | async-done | bytes 1310736 | tf_op jit(solution)/shard_map/all_gather | solution.py:110
  37.2 1.3 convolution_bitcast_fusion.3
  41.8 0.9 copy-done.1
  43.1 18.7 %all-gather.11.cloned.1.call-done = bf16[1280,512]{1,0:T(8,128)(2,1)} async-done(((bf16[160,512]{1,0:T(8,128)(2,1)}), bf16[1280,512]{1,0:T(8,128)(2,1)}) %all-gather.11.cloned.1.call-update) | async-done | bytes 1310736 | tf_op jit(solution)/shard_map/all_gather | solution.py:111
  61.8 1.4 fusion.14
  63.3 1.3 fusion.13
  65.3 3.0 convolution_convert_fusion.3
  69.8 0.9 reduce-window.6
  71.4 12.7 %reduce-scatter.2.cloned.1.call-done = bf16[80,2048]{1,0:T(8,128)(2,1)} async-done(((bf16[160,2048]{1,0:T(8,128)(2,1)}), bf16[80,2048]{1,0:T(8,128)(2,1)}) %reduce-scatter.2.cloned.1.call-update) | async-done | bytes 327696 | tf_op jit(solution)/shard_map/reduce_scatter | solution.py:147
  84.1 1.2 fusion.23
  85.3 1.7 convolution_convert_fusion.2
  87.0 1.6 reshape.371
  88.6 4.6 %all-to-all-start = ((bf16[8,60,2048]{2,1,0:T(8,128)(2,1)}), bf16[8,60,2048]{2,1,0:T(8,128)(2,1)S(1)}, u32[]{:S(2)}, u32[]{:S(2)}) async-start(bf16[8,60,2048]{2,1,0:T(8,128)(2,1)} %reshape.371), calls=%async_computation.1 | async-start | bytes 4194304 | tf_op jit(solution)/shard_map/all_to_all | solution.py:183
  93.8 48.5 %all-to-all-done = bf16[8,60,2048]{2,1,0:T(8,128)(2,1)S(1)} async-done(((bf16[8,60,2048]{2,1,0:T(8,128)(2,1)}), bf16[8,60,2048]{2,1,0:T(8,128)(2,1)S(1)}, u32[]{:S(2)}, u32[]{:S(2)}) %all-to-all-start) | async-done | bytes 1966112 | tf_op jit(solution)/shard_map/all_to_all | solution.py:183
  142.2 1.5 reshape.372
  143.7 6.4 %fusion = f32[480,1024]{1,0:T(8,128)} fusion(bf16[480,2048]{1,0:T(8,128)(2,1)} %reshape.372, bf16[1,2048,1024]{2,1,0:T(8,128)(2,1)} %all-gather.15.cloned.1.call-done), kind=kOutput, calls=%fused_computation.1 | convolution fusion | flops 2013265920 | bytes 8126464 | tf_op jit(solution)/shard_map/dot_general | solution.py:51
  150.1 50.3 %all-gather.13.cloned.1.call-done = bf16[1,2048,1024]{2,1,0:T(8,128)(2,1)} async-done(((bf16[1,2048,512]{2,1,0:T(8,128)(2,1)}), bf16[1,2048,1024]{2,1,0:T(8,128)(2,1)}) %all-gather.13.cloned.1.call-update) | async-done | bytes 4194320 | tf_op jit(solution)/shard_map/all_gather | solution.py:180
  200.4 6.5 %multiply_convert_fusion = bf16[480,1024]{1,0:T(8,128)(2,1)} fusion(f32[480,1024]{1,0:T(8,128)} %fusion, bf16[480,2048]{1,0:T(8,128)(2,1)S(1)} %copy-done.5, bf16[1,2048,1024]{2,1,0:T(8,128)(2,1)} %all-gather.13.cloned.1.call-done), kind=kOutput, calls=%fused_computation.26 | convolution fusion | flops 2018181120 | bytes 9109504 | tf_op jit(solution)/shard_map/dot_general | solution.py:52
  206.9 51.7 %all-gather.17.cloned.1.call-done = bf16[1,1024,2048]{2,1,0:T(8,128)(2,1)} async-done(((bf16[1,512,2048]{2,1,0:T(8,128)(2,1)}), bf16[1,1024,2048]{2,1,0:T(8,128)(2,1)}) %all-gather.17.cloned.1.call-update) | async-done | bytes 4194320 | tf_op jit(solution)/shard_map/all_gather | solution.py:181
  258.6 3.1 convolution_convert_fusion
  261.8 1.2 add_convert_fusion
  263.0 1.5 reshape.373
  264.5 4.7 %all-to-all-start.1 = ((bf16[8,60,2048]{2,1,0:T(8,128)(2,1)}), bf16[8,60,2048]{2,1,0:T(8,128)(2,1)}, u32[]{:S(2)}, u32[]{:S(2)}) async-start(bf16[8,60,2048]{2,1,0:T(8,128)(2,1)} %reshape.373), calls=%async_computation.2 | async-start | bytes 4194304 | tf_op jit(solution)/shard_map/all_to_all | solution.py:187
  269.5 48.9 %all-to-all-done.1 = bf16[8,60,2048]{2,1,0:T(8,128)(2,1)} async-done(((bf16[8,60,2048]{2,1,0:T(8,128)(2,1)}), bf16[8,60,2048]{2,1,0:T(8,128)(2,1)}, u32[]{:S(2)}, u32[]{:S(2)}) %all-to-all-start.1) | async-done | bytes 1966112 | tf_op jit(solution)/shard_map/all_to_all | solution.py:187
  318.4 1.7 reshape.374
  320.1 3.0 gather_fusion
  323.2 2.6 reshape.378
  325.8 1.9 multiply_reduce_fusion
  (97 shorter events, 10.0 us)
Async XLA Ops:
  6.5 1.9 copy-start
  6.5 6.0 %copy-start.10 = (bf16[160,64]{0,1:T(8,128)(2,1)S(1)}, bf16[160,64]{0,1:T(8,128)(2,1)}, u32[]{:S(2)}) copy-start(bf16[160,64]{0,1:T(8,128)(2,1)} %param.18) | copy-start | bytes 61444
  6.5 6.0 %copy-start.9 = (bf16[160,256]{1,0:T(8,128)(2,1)S(1)}, bf16[160,256]{1,0:T(8,128)(2,1)}, u32[]{:S(2)}) copy-start(bf16[160,256]{1,0:T(8,128)(2,1)} %param.16) | copy-start | bytes 245764
  6.5 23.0 %copy-start.8 = (bf16[160,512]{1,0:T(8,128)(2,1)S(1)}, bf16[160,512]{1,0:T(8,128)(2,1)}, u32[]{:S(2)}) copy-start(bf16[160,512]{1,0:T(8,128)(2,1)} %param.15) | copy-start | bytes 491524
  6.5 30.7 %all-gather.9.cloned.1.call-start = ((), (), s32[]{:S(2)}) async-start(), calls=%async_computation.3 | async-start | bytes 1474560 | tf_op jit(solution)/shard_map/all_gather | solution.py:110
  10.3 51.6 %all-gather.11.cloned.1.call-start = ((), (), s32[]{:S(2)}) async-start(), calls=%async_computation.4 | async-start | bytes 1474560 | tf_op jit(solution)/shard_map/all_gather | solution.py:111
  12.4 71.7 %reduce-scatter.2.cloned.1.call-start = ((), (), s32[]{:S(2)}) async-start(), calls=%async_computation.5 | async-start | bytes 983040 | tf_op jit(solution)/shard_map/reduce_scatter | solution.py:147
  37.2 1.8 copy-start.6
  41.8 0.9 copy-start.1
  61.8 2.8 copy-start.7
  61.8 3.1 copy-start.2
  68.3 1.2 copy-start.12
  68.3 2.9 copy-start.11
  68.4 15.7 %copy-start.3 = (bf16[80,2048]{1,0:T(8,128)(2,1)S(1)}, bf16[80,2048]{1,0:T(8,128)(2,1)}, u32[]{:S(2)}) copy-start(bf16[80,2048]{1,0:T(8,128)(2,1)} %param.22) | copy-start | bytes 983044
  68.4 75.3 %all-gather.15.cloned.1.call-start = ((), (), s32[]{:S(2)}) async-start(), calls=%async_computation.7 | async-start | bytes 6291456 | tf_op jit(solution)/shard_map/all_gather | solution.py:179
  68.9 131.5 %all-gather.13.cloned.1.call-start = ((), (), s32[]{:S(2)}) async-start(), calls=%async_computation.6 | async-start | bytes 6291456 | tf_op jit(solution)/shard_map/all_gather | solution.py:180
  88.6 53.6 %all-to-all-start = ((bf16[8,60,2048]{2,1,0:T(8,128)(2,1)}), bf16[8,60,2048]{2,1,0:T(8,128)(2,1)S(1)}, u32[]{:S(2)}, u32[]{:S(2)}) async-start(bf16[8,60,2048]{2,1,0:T(8,128)(2,1)} %reshape.371), calls=%async_computation.1 | async-start | bytes 4194304 | tf_op jit(solution)/shard_map/all_to_all | solution.py:183
  93.2 165.4 %all-gather.17.cloned.1.call-start = ((), (), s32[]{:S(2)}) async-start(), calls=%async_computation.8 | async-start | bytes 6291456 | tf_op jit(solution)/shard_map/all_gather | solution.py:181
  143.7 56.7 %copy-start.5 = (bf16[480,2048]{1,0:T(8,128)(2,1)S(1)}, bf16[480,2048]{1,0:T(8,128)(2,1)}, u32[]{:S(2)}) copy-start(bf16[480,2048]{1,0:T(8,128)(2,1)} %reshape.372) | copy-start | bytes 5898244
  258.6 3.1 copy-start.14
  258.6 3.2 copy-start.15
  264.5 4.8 %copy-start.13 = (f32[80,4]{0,1:T(4,128)S(1)}, f32[80,4]{0,1:T(4,128)}, u32[]{:S(2)}) copy-start(f32[80,4]{0,1:T(4,128)} %param.29) | copy-start | bytes 3844
  264.5 53.9 %all-to-all-start.1 = ((bf16[8,60,2048]{2,1,0:T(8,128)(2,1)}), bf16[8,60,2048]{2,1,0:T(8,128)(2,1)}, u32[]{:S(2)}, u32[]{:S(2)}) async-start(bf16[8,60,2048]{2,1,0:T(8,128)(2,1)} %reshape.373), calls=%async_computation.2 | async-start | bytes 4194304 | tf_op jit(solution)/shard_map/all_to_all | solution.py:187
  325.8 1.9 copy-start.4
Sparse Core Ops, SparseCore 0:
  10.4 26.7 all-gather.8
  38.9 22.9 all-gather.10
  68.5 15.5 reduce-scatter.1
  85.5 56.7 all-gather.14
  143.6 56.7 all-gather.12
  201.8 56.7 all-gather.16
where the time goes:
time: 336 us; the launch traced here: 335 us
  waiting for transfers between devices  239 us (71%)
  matrix products  33 us (10%)
  blocking collectives  16.3 us (5%)
  local copies, waits for them, and re-layouts  14.6 us (4%)
  between operations  13.9 us (4%)
  starting transfers between devices  9.75 us (3%)
  other arithmetic  8.39 us (2%)
    all_gather x1, waiting for transfers between devices, on_device(): lax.all_gather(down_w, 'tp', axis=0, tiled=True)  51.7 us
    all_gather x1, waiting for transfers between devices, on_device(): lax.all_gather(up_w, 'tp', axis=1, tiled=True)  50.3 us
    all_to_all x1, waiting for transfers between devices, on_device(): lax.all_to_all(result_rows.reshape(experts_all, capacity, model_width), '...  48.9 us
    all_to_all x1, waiting for transfers between devices, on_device(): lax.all_to_all(outgoing, 'sp', split_axis=0, concat_axis=0, tiled=True)  48.5 us
    all_gather x1, waiting for transfers between devices, on_device(): piece_values = lax.all_gather(values, 'sp', axis=0, tiled=True)  18.7 us
    all_gather x1, blocking collectives, on_device(): piece_pairs = lax.all_gather(key_pairs, 'sp', axis=0, tiled=True)  16.3 us
    reduce_scatter x1, waiting for transfers between devices, on_device(): lax.psum_scatter(jnp.dot(attended, own_rows, preferred_element_type=jnp.f...  12.7 us
    all_gather x1, waiting for transfers between devices, on_device(): piece_keys = lax.all_gather(key_plain, 'sp', axis=0, tiled=True)  7.27 us
  transfers between devices with their start and end apart: 8, of which 7 were waited for; matrix products, arithmetic and copies ran while one was open for 9% of the time, Pallas kernels for 0%

commit v1 on v0

--- a/solution.py
+++ b/solution.py
@@ -11,6 +11,13 @@
 eps = 1e-06
 limit = 7.0
 slope = 1.702
+
+
+def all_by_exchange(x, axis, dim):
+    devices = lax.axis_size(axis)
+    blocks = jnp.stack([x for _ in range(devices)])
+    blocks = lax.all_to_all(blocks, axis, split_axis=0, concat_axis=0)
+    return jnp.concatenate(blocks, axis=dim)
 
 
 def turn(vector, row_shift, col_shift):
@@ -178,7 +185,7 @@
     gate_full, up_full, down_full = (
         lax.all_gather(gate_w, "tp", axis=1, tiled=True),
         lax.all_gather(up_w, "tp", axis=1, tiled=True),
-        lax.all_gather(down_w, "tp", axis=0, tiled=True),
+        all_by_exchange(down_w, "tp", 0),
     )
     arrived = lax.all_to_all(outgoing, "sp", split_axis=0, concat_axis=0, tiled=True)
     result_rows = expert_whole(

time: 336 us -> 325 us (0.967)
  waiting for transfers between devices: 239 us -> 216 us
  starting transfers between devices: 9.75 us -> 15.1 us
  other arithmetic: 8.39 us -> 13.4 us
    all_gather x1 -> x0, waiting for transfers between devices: 51.7 us -> none  [on_device(): lax.all_gather(down_w, 'tp', axis=0, tiled=True)]
    all_gather x1, waiting for transfers between devices: 50.3 us -> 83.5 us  [on_device(): lax.all_gather(up_w, 'tp', axis=1, tiled=True)]
    all_to_all x0 -> x1, starting transfers between devices: none -> 5.8 us  [all_by_exchange(): blocks = lax.all_to_all(blocks, axis, split_axis=0, concat_axis=0)]
    all_to_all x1, waiting for transfers between devices: 48.5 us -> 43.5 us  [on_device(): lax.all_to_all(outgoing, 'sp', split_axis=0, concat_axis=0, tiled=True)]
    another operation x5 -> x6, other arithmetic: 1.03 us -> 5.99 us  [the longest x1 4.96 us: all_by_exchange(): blocks = jnp.stack([x for _ in range(devices)])]
  transfers between devices with their start and end apart: 8 -> 8, of which waited for: 7 -> 6; matrix products, arithmetic and copies ran while one was open for 9% -> 11% of each run, Pallas kernels for 0% -> 0%
where the time goes in v1:
time: 325 us; the launch traced here: 324 us
  waiting for transfers between devices  216 us (66%)
  matrix products  35.4 us (11%)
  blocking collectives  16.3 us (5%)
  starting transfers between devices  15.1 us (5%)
  local copies, waits for them, and re-layouts  14.6 us (4%)
  between operations  13.6 us (4%)
  other arithmetic  13.4 us (4%)
    all_gather x1, waiting for transfers between devices, on_device(): lax.all_gather(up_w, 'tp', axis=1, tiled=True)  83.5 us
    all_to_all x1, waiting for transfers between devices, on_device(): lax.all_to_all(result_rows.reshape(experts_all, capacity, model_width), '...  48.8 us
    all_to_all x1, waiting for transfers between devices, on_device(): lax.all_to_all(outgoing, 'sp', split_axis=0, concat_axis=0, tiled=True)  43.5 us
    all_gather x1, waiting for transfers between devices, on_device(): piece_values = lax.all_gather(values, 'sp', axis=0, tiled=True)  18.7 us
    all_gather x1, blocking collectives, on_device(): piece_pairs = lax.all_gather(key_pairs, 'sp', axis=0, tiled=True)  16.3 us
    reduce_scatter x1, waiting for transfers between devices, on_device(): lax.psum_scatter(jnp.dot(attended, own_rows, preferred_element_type=jnp.f...  13.3 us
    all_gather x1, waiting for transfers between devices, on_device(): piece_keys = lax.all_gather(key_plain, 'sp', axis=0, tiled=True)  7.27 us
    dot_general x1, matrix products, expert_active(): jnp.dot(rows, gate_w, preferred_element_type=jnp.float32)  7.26 us
  transfers between devices with their start and end apart: 8, of which 6 were waited for; matrix products, arithmetic and copies ran while one was open for 11% of the time, Pallas kernels for 0%

profile of v1, /device:TPU:0, one launch (start us, length us, event | category | flops | bytes accessed | tf_op | source)
XLA Modules:
  0.0 324.4 jit_solution(773207930126809901)
XLA Ops:
  6.6 1.1 fusion.38
  8.4 1.9 convolution_convert_fusion.5
  10.3 2.1 convolution_convert_fusion.4
  13.1 16.3 %all_gather.16 = bf16[640,128]{1,0:T(8,128)(2,1)S(1)} all-gather(bf16[80,128]{1,0:T(8,128)(2,1)S(1)} %convert_element_type.125), channel_id=1, replica_groups=mesh['grp'=2,'sp'=8,'tp'=2] {'sp'}, dimensions={0}, use_global_device_ids=true | all-gather | bytes 184320 | tf_op jit(solution)/shard_map/all_gather | solution.py:119
  30.0 7.3 %all-gather.7.cloned.1.call-done = bf16[1280,512]{1,0:T(8,128)(2,1)} async-done(((bf16[160,512]{1,0:T(8,128)(2,1)}), bf16[1280,512]{1,0:T(8,128)(2,1)}) %all-gather.7.cloned.1.call-update) | async-done | bytes 1310736 | tf_op jit(solution)/shard_map/all_gather | solution.py:117
  37.2 1.3 convolution_bitcast_fusion.3
  41.8 0.9 copy-done.2
  43.1 18.7 %all-gather.9.cloned.1.call-done = bf16[1280,512]{1,0:T(8,128)(2,1)} async-done(((bf16[160,512]{1,0:T(8,128)(2,1)}), bf16[1280,512]{1,0:T(8,128)(2,1)}) %all-gather.9.cloned.1.call-update) | async-done | bytes 1310736 | tf_op jit(solution)/shard_map/all_gather | solution.py:118
  61.8 1.4 fusion.14
  63.3 1.3 fusion.13
  65.3 3.0 convolution_convert_fusion.3
  70.8 13.3 %reduce-scatter.2.cloned.1.call-done = bf16[80,2048]{1,0:T(8,128)(2,1)} async-done(((bf16[160,2048]{1,0:T(8,128)(2,1)}), bf16[80,2048]{1,0:T(8,128)(2,1)}) %reduce-scatter.2.cloned.1.call-update) | async-done | bytes 327696 | tf_op jit(solution)/shard_map/reduce_scatter | solution.py:154
  84.1 1.2 fusion.23
  85.3 1.7 convolution_convert_fusion.2
  87.0 1.6 reshape.374
  88.6 4.6 %all-to-all-start = ((bf16[8,60,2048]{2,1,0:T(8,128)(2,1)}), bf16[8,60,2048]{2,1,0:T(8,128)(2,1)S(1)}, u32[]{:S(2)}, u32[]{:S(2)}) async-start(bf16[8,60,2048]{2,1,0:T(8,128)(2,1)} %reshape.374), calls=%async_computation.1 | async-start | bytes 4194304 | tf_op jit(solution)/shard_map/all_to_all | solution.py:190
  93.8 5.0 %pad_maximum_fusion = bf16[2,512,2048]{2,1,0:T(8,128)(2,1)} fusion(bf16[1,512,2048]{2,1,0:T(8,128)(2,1)} %param.27), kind=kLoop, calls=%fused_computation.1 | loop fusion | flops 2097152 | bytes 6291456 | tf_op jit(solution)/shard_map/stack | solution.py:18
  98.7 43.5 %all-to-all-done = bf16[8,60,2048]{2,1,0:T(8,128)(2,1)S(1)} async-done(((bf16[8,60,2048]{2,1,0:T(8,128)(2,1)}), bf16[8,60,2048]{2,1,0:T(8,128)(2,1)S(1)}, u32[]{:S(2)}, u32[]{:S(2)}) %all-to-all-start) | async-done | bytes 1966112 | tf_op jit(solution)/shard_map/all_to_all | solution.py:190
  142.2 5.8 %all-to-all-start.1 = ((bf16[2,512,2048]{2,1,0:T(8,128)(2,1)}), bf16[2,512,2048]{2,1,0:T(8,128)(2,1)}, u32[]{:S(2)}, u32[]{:S(2)}) async-start(bf16[2,512,2048]{2,1,0:T(8,128)(2,1)} %pad_maximum_fusion), calls=%async_computation.2 | async-start | bytes 8388608 | tf_op jit(solution)/shard_map/all_to_all | solution.py:19
  148.0 1.5 reshape.375
  149.5 7.3 %fusion = f32[480,1024]{1,0:T(8,128)} fusion(bf16[480,2048]{1,0:T(8,128)(2,1)} %reshape.375, bf16[1,2048,1024]{2,1,0:T(8,128)(2,1)} %all-gather.13.cloned.1.call-done), kind=kOutput, calls=%fused_computation.2 | convolution fusion | flops 2013265920 | bytes 8126464 | tf_op jit(solution)/shard_map/dot_general | solution.py:58
  156.8 83.5 %all-gather.11.cloned.1.call-done = bf16[1,2048,1024]{2,1,0:T(8,128)(2,1)} async-done(((bf16[1,2048,512]{2,1,0:T(8,128)(2,1)}), bf16[1,2048,1024]{2,1,0:T(8,128)(2,1)}) %all-gather.11.cloned.1.call-update) | async-done | bytes 4194320 | tf_op jit(solution)/shard_map/all_gather | solution.py:187
  240.3 6.4 %multiply_convert_fusion = bf16[480,1024]{1,0:T(8,128)(2,1)} fusion(f32[480,1024]{1,0:T(8,128)} %fusion, bf16[480,2048]{1,0:T(8,128)(2,1)S(1)} %copy-done.6, bf16[1,2048,1024]{2,1,0:T(8,128)(2,1)} %all-gather.11.cloned.1.call-done), kind=kOutput, calls=%fused_computation.27 | convolution fusion | flops 2018181120 | bytes 9109504 | tf_op jit(solution)/shard_map/dot_general | solution.py:59
  246.7 3.0 convolution_convert_fusion
  249.8 2.8 add_convert_fusion
  252.6 1.5 reshape.376
  254.1 4.5 %all-to-all-start.2 = ((bf16[8,60,2048]{2,1,0:T(8,128)(2,1)}), bf16[8,60,2048]{2,1,0:T(8,128)(2,1)}, u32[]{:S(2)}, u32[]{:S(2)}) async-start(bf16[8,60,2048]{2,1,0:T(8,128)(2,1)} %reshape.376), calls=%async_computation.3 | async-start | bytes 4194304 | tf_op jit(solution)/shard_map/all_to_all | solution.py:194
  258.8 48.8 %all-to-all-done.2 = bf16[8,60,2048]{2,1,0:T(8,128)(2,1)} async-done(((bf16[8,60,2048]{2,1,0:T(8,128)(2,1)}), bf16[8,60,2048]{2,1,0:T(8,128)(2,1)}, u32[]{:S(2)}, u32[]{:S(2)}) %all-to-all-start.2) | async-done | bytes 1966112 | tf_op jit(solution)/shard_map/all_to_all | solution.py:194
  307.6 1.7 reshape.377
  309.4 3.0 gather_fusion
  312.4 2.7 reshape.381
  315.1 1.9 multiply_reduce_fusion
  (97 shorter events, 10.3 us)
Async XLA Ops:
  6.5 1.9 copy-start
  6.5 6.0 %copy-start.11 = (bf16[160,64]{0,1:T(8,128)(2,1)S(1)}, bf16[160,64]{0,1:T(8,128)(2,1)}, u32[]{:S(2)}) copy-start(bf16[160,64]{0,1:T(8,128)(2,1)} %param.18) | copy-start | bytes 61444
  6.5 6.0 %copy-start.10 = (bf16[160,256]{1,0:T(8,128)(2,1)S(1)}, bf16[160,256]{1,0:T(8,128)(2,1)}, u32[]{:S(2)}) copy-start(bf16[160,256]{1,0:T(8,128)(2,1)} %param.16) | copy-start | bytes 245764
  6.5 23.0 %copy-start.9 = (bf16[160,512]{1,0:T(8,128)(2,1)S(1)}, bf16[160,512]{1,0:T(8,128)(2,1)}, u32[]{:S(2)}) copy-start(bf16[160,512]{1,0:T(8,128)(2,1)} %param.15) | copy-start | bytes 491524
  6.5 30.7 %all-gather.7.cloned.1.call-start = ((), (), s32[]{:S(2)}) async-start(), calls=%async_computation.4 | async-start | bytes 1474560 | tf_op jit(solution)/shard_map/all_gather | solution.py:117
  10.3 51.6 %all-gather.9.cloned.1.call-start = ((), (), s32[]{:S(2)}) async-start(), calls=%async_computation.5 | async-start | bytes 1474560 | tf_op jit(solution)/shard_map/all_gather | solution.py:118
  12.4 71.7 %reduce-scatter.2.cloned.1.call-start = ((), (), s32[]{:S(2)}) async-start(), calls=%async_computation.6 | async-start | bytes 983040 | tf_op jit(solution)/shard_map/reduce_scatter | solution.py:154
  37.2 1.8 copy-start.7
  41.8 0.9 copy-start.2
  61.8 2.8 copy-start.8
  61.8 3.1 copy-start.3
  68.3 0.7 copy-start.13
  68.3 2.3 copy-start.12
  68.3 15.8 %copy-start.4 = (bf16[80,2048]{1,0:T(8,128)(2,1)S(1)}, bf16[80,2048]{1,0:T(8,128)(2,1)}, u32[]{:S(2)}) copy-start(bf16[80,2048]{1,0:T(8,128)(2,1)} %param.22) | copy-start | bytes 983044
  68.3 81.2 %all-gather.13.cloned.1.call-start = ((), (), s32[]{:S(2)}) async-start(), calls=%async_computation.8 | async-start | bytes 6291456 | tf_op jit(solution)/shard_map/all_gather | solution.py:186
  88.6 53.6 %all-to-all-start = ((bf16[8,60,2048]{2,1,0:T(8,128)(2,1)}), bf16[8,60,2048]{2,1,0:T(8,128)(2,1)S(1)}, u32[]{:S(2)}, u32[]{:S(2)}) async-start(bf16[8,60,2048]{2,1,0:T(8,128)(2,1)} %reshape.374), calls=%async_computation.1 | async-start | bytes 4194304 | tf_op jit(solution)/shard_map/all_to_all | solution.py:190
  93.2 147.1 %all-gather.11.cloned.1.call-start = ((), (), s32[]{:S(2)}) async-start(), calls=%async_computation.7 | async-start | bytes 6291456 | tf_op jit(solution)/shard_map/all_gather | solution.py:187
  142.2 104.5 %all-to-all-start.1 = ((bf16[2,512,2048]{2,1,0:T(8,128)(2,1)}), bf16[2,512,2048]{2,1,0:T(8,128)(2,1)}, u32[]{:S(2)}, u32[]{:S(2)}) async-start(bf16[2,512,2048]{2,1,0:T(8,128)(2,1)} %pad_maximum_fusion), calls=%async_computation.2 | async-start | bytes 8388608 | tf_op jit(solution)/shard_map/all_to_all | solution.py:19
  149.5 90.8 %copy-start.6 = (bf16[480,2048]{1,0:T(8,128)(2,1)S(1)}, bf16[480,2048]{1,0:T(8,128)(2,1)}, u32[]{:S(2)}) copy-start(bf16[480,2048]{1,0:T(8,128)(2,1)} %reshape.375) | copy-start | bytes 5898244
  246.7 3.0 copy-start.15
  254.1 4.6 %copy-start.14 = (f32[80,4]{0,1:T(4,128)S(1)}, f32[80,4]{0,1:T(4,128)}, u32[]{:S(2)}) copy-start(f32[80,4]{0,1:T(4,128)} %param.29) | copy-start | bytes 3844
  254.1 53.5 %all-to-all-start.2 = ((bf16[8,60,2048]{2,1,0:T(8,128)(2,1)}), bf16[8,60,2048]{2,1,0:T(8,128)(2,1)}, u32[]{:S(2)}, u32[]{:S(2)}) async-start(bf16[8,60,2048]{2,1,0:T(8,128)(2,1)} %reshape.376), calls=%async_computation.3 | async-start | bytes 4194304 | tf_op jit(solution)/shard_map/all_to_all | solution.py:194
  312.4 5.5 %copy-start.1 = (bf16[512,512]{1,0:T(8,128)(2,1)S(1)}, bf16[512,512]{1,0:T(8,128)(2,1)}, u32[]{:S(2)}) copy-start(bf16[512,512]{1,0:T(8,128)(2,1)} %param.20) | copy-start | bytes 1572868
  315.1 1.9 copy-start.5
Sparse Core Ops, SparseCore 0:
  10.4 26.7 all-gather.6
  38.9 22.9 all-gather.8
  68.4 15.5 reduce-scatter.1
  85.5 56.7 all-gather.12
  143.6 96.5 all-gather.10
